TPU v7x, 32 devices: a whole 2x2x4 slice. The times are simulated.
32 devices in a mesh: grp: 2 (over y), ep: 8 (over z, x), tp: 2 (over core).
Axes of the slice: x: 2, y: 2, z: 4, core: 2. Of those that a mesh axis runs over, the one named last changes fastest.
Arguments:
- tokens: bfloat16 [2048, 2048], P(('grp', 'ep')), parts along dimension 0, may hold values from -6 to 6
- in_gain: float32 [2048], replicated, may hold values from 0.1 to 1.9
- routing: int32 [2048, 4], P(('grp', 'ep')), parts along dimension 0, may hold values from 0 to 15, as said below
- gate_prob: float32 [2048, 4], P(('grp', 'ep')), parts along dimension 0, may hold values from 0.05 to 1
- w_gate: bfloat16 [16, 2048, 512], P('ep', None, 'tp'), may hold values from -0.125 to 0.125
- w_up: bfloat16 [16, 2048, 512], P('ep', None, 'tp'), may hold values from -0.125 to 0.125
- w_down: bfloat16 [16, 512, 2048], P('ep', 'tp')
- out_gain: float32 [2048], P('tp'), may hold values from 0.1 to 1.9
Outputs:
- output: bfloat16 [2048, 2048], P(('grp', 'ep'), 'tp'), parts along dimension 0
There are 2 independent parts, one for each index of `grp`. A program takes and returns all parts, laid end to end along the dimension named above; an argument that names none is the same for every part. Nothing has to cross between parts.
Inputs may be any that keep to these rules, and one draw needn't show every extreme that they name: `routing`: each row names 4 different experts, all of one group (the same value of expert // 4). In the rows of one device no expert is named more than 64 times, and in every device's rows some expert is named exactly 64 times.
All inputs are finite; a program needn't handle non-finite values.
Results may differ from a plain program's by a relative error of at most 0.0077.
Values may be sent and summed in bfloat16 or wider, within the bound.
A program may use at most 64 MiB of HBM per device.

v0:
```python
import functools

import jax
import jax.numpy as jnp
from jax import lax
from jax.experimental import pallas as pl
from jax.experimental.pallas import tpu as pltpu
from jax.sharding import PartitionSpec as P

GROUPS = 4
EPS = 1e-06
CHUNKS = 2
MESH = pl.DeviceIdType.MESH
F32 = jnp.float32
BF16 = jnp.bfloat16


def loop(low, high, step):
    if high - low <= 8:
        for i in range(low, high):
            step(i)
    else:
        lax.fori_loop(low, high, lambda i, carry: (step(i), carry)[1], 0)


def kernel(
    group_count, span, rows,
    routes_ref, probs_ref, in_gain_ref, out_gain_ref, tokens_hbm, gate_hbm, up_hbm, down_hbm,
    out_ref,
    tokens_ref, sendz, gathered, unpack, gate_send, gate_recv, w_gate, w_up, w_down, hidden,
    kept, tp_send, tp_recv, own_sum, grp_recv, home_send, home_recv, sq_send, sq_recv,
    tok_sem, w_sem, gate_ss, gate_rs, z_ss, z_rs, x_ss, x_rs, t_ss, t_rs, p_ss, p_rs, r_ss, r_rs, h_ss, h_rs, q_ss, q_rs,
):
    Q, S, R = group_count, span, rows
    N = Q * S
    K = CHUNKS
    RC = R // K
    top, tok = routes_ref.shape
    width = tokens_ref.shape[1]
    H = out_ref.shape[1]
    L, _, F = gate_hbm.shape
    group_width = S * L
    gate_rows, lanes = gate_send.shape[1:]
    me = lax.axis_index("ep")
    c = lax.axis_index("tp")
    q, s = me // S, lax.rem(me, S)
    order = [0] + sorted(range(1, Q), key=lambda d: -min(d, Q - d))

    def at(ep, tp=None):
        return {"ep": ep, "tp": c if tp is None else tp}

    def remote(src, dst, ss, rs, dev):
        return pltpu.make_async_remote_copy(
            src_ref=src, dst_ref=dst, send_sem=ss, recv_sem=rs, device_id=dev, device_id_type=MESH
        )

    tok_copy = pltpu.make_async_copy(tokens_hbm, tokens_ref, tok_sem)
    tok_copy.start()

    barrier = pltpu.get_barrier_semaphore()
    loop(1, N, lambda p: pl.semaphore_signal(
        barrier, inc=1, device_id=at(lax.rem(me + p, N)), device_id_type=MESH))
    pl.semaphore_signal(barrier, inc=1, device_id=at(me, 1 - c), device_id_type=MESH)

    weights = []
    for n, (src, dst) in enumerate(((gate_hbm, w_gate), (up_hbm, w_up), (down_hbm, w_down))):
        for e in range(L):
            weights.append(pltpu.make_async_copy(src.at[e], dst.at[e], w_sem.at[n, e]))
    for copy in weights:
        copy.start()

    first = routes_ref[0:1, :]
    groups = lax.broadcasted_iota(jnp.int32, (16, tok), 0)
    member = (first >= groups * group_width) & (first < (groups + 1) * group_width)
    earlier = lax.broadcasted_iota(jnp.int32, (tok, tok), 0) < lax.broadcasted_iota(jnp.int32, (tok, tok), 1)
    rank = jnp.dot(
        jnp.where(member, 1.0, 0.0).astype(BF16), jnp.where(earlier, 1.0, 0.0).astype(BF16),
        preferred_element_type=F32,
    ).astype(jnp.int32)
    slots = lax.broadcasted_iota(jnp.int32, (lanes, tok), 0)
    picks = []
    for g in range(Q):
        inside = (first >= g * group_width) & (first < (g + 1) * group_width)
        picks.append(jnp.where((rank[g:g + 1, :] == slots) & inside, 1.0, 0.0))

    tok_copy.wait()
    floats = tokens_ref[...].astype(F32)
    inv = lax.rsqrt(jnp.mean(floats * floats, axis=-1, keepdims=True) + EPS)
    own_cols = pl.ds(pl.multiple_of(c * H, H), H)
    other_cols = pl.ds(pl.multiple_of((1 - c) * H, H), H)
    normed = (tokens_ref[:, own_cols].astype(F32) * inv * in_gain_ref[:, own_cols]).astype(BF16)
    for g in range(Q):
        sendz[g] = jnp.dot(
            picks[g][:R].astype(BF16), normed, preferred_element_type=F32
        ).astype(BF16)

    gathered[q, s, c] = sendz[q]
    pl.semaphore_wait(barrier, N)

    def z_copy(d, k):
        to = lax.rem(q + d, Q)
        part = pl.ds(k * RC, RC)
        return remote(
            sendz.at[to, part], gathered.at[q, s, c, part], z_ss.at[d, k], z_rs.at[d, k], at(to * S + s)
        )

    def source(d):
        return lax.rem(q + Q - d, Q)

    def x_copy(d, e, k):
        block = gathered.at[source(d), s, c, pl.ds(k * RC, RC)]
        return remote(block, block, x_ss.at[d, e, k], x_rs.at[d, e, k], at(q * S + lax.rem(s + e, S)))

    def t_copy(d, e, k):
        block = gathered.at[source(d), lax.rem(s + S - e, S), c, pl.ds(k * RC, RC)]
        return remote(block, block, t_ss.at[d, e, k], t_rs.at[d, e, k], at(me, 1 - c))

    def gate_copy(d, e):
        to_q, to_s = lax.rem(q + d, Q), lax.rem(s + e, S)
        return remote(
            gate_send.at[to_q], gate_recv.at[me], gate_ss.at[d, e], gate_rs.at[d, e], at(to_q * S + to_s)
        )

    def p_copy(d):
        return remote(tp_send.at[d], tp_recv.at[d], p_ss.at[d], p_rs.at[d], at(me, 1 - c))

    def r_copy(d, e, k):
        to = lax.rem(s + e, S)
        part = pl.ds(k * RC, RC)
        return remote(
            tp_send.at[d, to, part], grp_recv.at[d, e, part], r_ss.at[d, e, k], r_rs.at[d, e, k], at(q * S + to)
        )

    def h_copy(d, k):
        part = pl.ds(k * RC, RC)
        return remote(
            home_send.at[d, part], home_recv.at[q, part], h_ss.at[d, k], h_rs.at[d, k], at(source(d) * S + s)
        )

    def forward(d, k):
        loop(1, S, lambda e: x_copy(d, e, k).start())
        t_copy(d, 0, k).start()

    for k in range(K):
        forward(0, k)
    for k in range(K):
        z_copy(order[1], k).start()

    for g in range(Q):
        ids = g * group_width + lax.broadcasted_iota(jnp.int32, (gate_rows, tok), 0)
        dense = jnp.zeros((gate_rows, tok), F32)
        for k in range(top):
            dense += jnp.where(routes_ref[k:k + 1, :] == ids, probs_ref[k:k + 1, :], 0.0)
        gate_send[g] = lax.dot_general(
            dense, picks[g], (((1,), (1,)), ((), ())),
            precision=lax.Precision.HIGHEST, preferred_element_type=F32,
        )
    gate_recv[me] = gate_send[q]

    for d in order:
        loop(1 if d == 0 else 0, S, lambda e: gate_copy(d, e).start())
    for d in order[2:]:
        for k in range(K):
            z_copy(d, k).start()

    unpack[...] = jnp.concatenate([pick[:R] for pick in picks], axis=0).T.astype(BF16)

    def stage_a(d):
        for k in range(K):
            z_copy(d, k).wait_recv()
            forward(d, k)

    def stage_b(d):
        for k in range(K):
            def one(e):
                x_copy(d, e, k).wait_recv()
                t_copy(d, e, k).start()
            loop(1, S, one)

    pair = 2 if S % 2 == 0 else 1

    def stage_c(d):
        loop(1 if d == 0 else 0, S, lambda e: gate_copy(d, e).wait_recv())
        for k in range(K):
            loop(0, S, lambda e: t_copy(d, e, k).wait_recv())
        src = source(d)
        diagonal = (
            lax.broadcasted_iota(jnp.int32, (R, lanes), 0) == lax.broadcasted_iota(jnp.int32, (R, lanes), 1)
        )

        def some(n):
            base = n * pair
            low = gathered[src, pl.ds(base, pair), 0].reshape(pair * R, H)
            high = gathered[src, pl.ds(base, pair), 1].reshape(pair * R, H)
            for j in range(L):
                gate = jnp.dot(low, w_gate[j, :H], preferred_element_type=F32)
                gate += jnp.dot(high, w_gate[j, H:], preferred_element_type=F32)
                up = jnp.dot(low, w_up[j, :H], preferred_element_type=F32)
                up += jnp.dot(high, w_up[j, H:], preferred_element_type=F32)
                scales = []
                for b in range(pair):
                    line = gate_recv[src * S + base + b, pl.ds(s * L + j, 1), :]
                    scales.append(jnp.sum(jnp.where(diagonal, line, 0.0), axis=1, keepdims=True))
                scale = jnp.concatenate(scales, axis=0)
                act = gate / (1.0 + jnp.exp(-gate)) * up
                hidden[:, j * F:(j + 1) * F] = (act * scale).astype(BF16)
            other = jnp.zeros((pair * R, H), F32)
            mine = jnp.zeros((pair * R, H), F32)
            for j in range(L):
                other += jnp.dot(hidden[:, j * F:(j + 1) * F], w_down[j, :, other_cols], preferred_element_type=F32)
            tp_send[d, pl.ds(base, pair)] = other.astype(BF16).reshape(pair, R, H)
            for j in range(L):
                mine += jnp.dot(hidden[:, j * F:(j + 1) * F], w_down[j, :, own_cols], preferred_element_type=F32)
            kept[min(d, 1), pl.ds(base, pair)] = mine.reshape(pair, R, H)

        if S == pair:
            some(0)
        else:
            lax.fori_loop(0, S // pair, lambda n, carry: (some(n), carry)[1], 0)
        p_copy(d).start()

    def stage_e(d):
        p_copy(d).wait()
        for k in range(K):
            part = pl.ds(k * RC, RC)

            def one(e):
                to = lax.rem(s + e, S)
                tp_send[d, to, part] = (kept[min(d, 1), to, part] + tp_recv[d, to, part].astype(F32)).astype(BF16)
                r_copy(d, e, k).start()
            loop(1, S, one)
        own_sum[d] = kept[min(d, 1), s] + tp_recv[d, s].astype(F32)

    def stage_f(d):
        for k in range(K):
            part = pl.ds(k * RC, RC)

            def one(e):
                r_copy(d, e, k).wait_recv()
                own_sum[d, part] += grp_recv[d, e, part].astype(F32)
            loop(1, S, one)
            if d == 0:
                home_recv[q, part] = own_sum[d, part].astype(BF16)
            else:
                home_send[d, part] = own_sum[d, part].astype(BF16)
                h_copy(d, k).start()

    stage_b(0)
    for i in range(Q):
        if i + 1 < Q:
            stage_a(order[i + 1])
        if i == 0:
            for copy in weights:
                copy.wait()
        if i >= 3:
            stage_f(order[i - 2])
        if i >= 2:
            stage_e(order[i - 1])
        stage_c(order[i])
        if i + 1 < Q:
            stage_b(order[i + 1])
    if Q >= 2:
        stage_e(order[Q - 1])
    stage_e(0)
    for d in order[max(1, Q - 2):]:
        stage_f(d)
    stage_f(0)

    for d in order[1:]:
        for k in range(K):
            h_copy(d, k).wait_recv()
    mixed = jnp.dot(unpack[...], home_recv[...].reshape(Q * R, H), preferred_element_type=F32)
    squares = jnp.sum(mixed * mixed, axis=1, keepdims=True)
    sq_send[...] = jnp.broadcast_to(squares, sq_send.shape)
    sq_copy = remote(sq_send, sq_recv, q_ss, q_rs, at(me, 1 - c))
    sq_copy.start()
    for d in range(Q):
        loop(1 if d == 0 else 0, S, lambda e: gate_copy(d, e).wait_send())
        for k in range(K):
            if d > 0:
                z_copy(d, k).wait_send()
                h_copy(d, k).wait_send()

            def sent(e):
                x_copy(d, e, k).wait_send()
                r_copy(d, e, k).wait_send()
            loop(1, S, sent)
            loop(0, S, lambda e: t_copy(d, e, k).wait_send())
    sq_copy.wait()
    total = squares + sq_recv[:, 0:1]
    out_ref[...] = (mixed * lax.rsqrt(total / width + EPS) * out_gain_ref[...]).astype(BF16)


def body(tokens, in_gain, routing, gate_prob, w_gate, w_up, w_down, out_gain):
    N = lax.axis_size("ep")
    L, D, F = w_gate.shape
    tok, top = routing.shape
    H = out_gain.shape[0]
    group_width = L * N // GROUPS
    cap = max(2, tok * top // (2 * group_width))
    R = min(tok, group_width * cap // top)
    R = -(-R // 16) * 16
    Q, S = GROUPS, N // GROUPS
    lanes = -(-R // 128) * 128
    gate_rows = -(-group_width // 8) * 8
    pair = 2 if S % 2 == 0 else 1
    vmem = pl.BlockSpec(memory_space=pltpu.VMEM)
    hbm = pl.BlockSpec(memory_space=pl.ANY)
    dma = pltpu.SemaphoreType.DMA
    return pl.pallas_call(
        functools.partial(kernel, Q, S, R),
        out_shape=jax.ShapeDtypeStruct((tok, H), BF16),
        in_specs=[vmem] * 4 + [hbm] * 4,
        out_specs=vmem,
        scratch_shapes=[
            pltpu.VMEM((tok, D), BF16),
            pltpu.VMEM((Q, R, H), BF16),
            pltpu.VMEM((Q, S, 2, R, H), BF16),
            pltpu.VMEM((tok, Q * R), BF16),
            pltpu.VMEM((Q, gate_rows, lanes), F32),
            pltpu.VMEM((N, gate_rows, lanes), F32),
            pltpu.VMEM((L, D, F), BF16),
            pltpu.VMEM((L, D, F), BF16),
            pltpu.VMEM((L, F, D), BF16),
            pltpu.VMEM((pair * R, L * F), BF16),
            pltpu.VMEM((2, S, R, H), F32),
            pltpu.VMEM((Q, S, R, H), BF16),
            pltpu.VMEM((Q, S, R, H), BF16),
            pltpu.VMEM((Q, R, H), F32),
            pltpu.VMEM((Q, S, R, H), BF16),
            pltpu.VMEM((Q, R, H), BF16),
            pltpu.VMEM((Q, R, H), BF16),
            pltpu.VMEM((tok, 128), F32),
            pltpu.VMEM((tok, 128), F32),
            dma, dma((3, L)), dma((Q, S)), dma((Q, S)), dma((Q, CHUNKS)), dma((Q, CHUNKS)),
            dma((Q, S, CHUNKS)), dma((Q, S, CHUNKS)), dma((Q, S, CHUNKS)), dma((Q, S, CHUNKS)),
            dma((Q,)), dma((Q,)), dma((Q, S, CHUNKS)), dma((Q, S, CHUNKS)), dma((Q, CHUNKS)), dma((Q, CHUNKS)),
            dma, dma,
        ],
        compiler_params=pltpu.CompilerParams(
            collective_id=0, has_side_effects=True, vmem_limit_bytes=64 * 1000 * 1000
        ),
    )(routing.T, gate_prob.T, in_gain.reshape(1, D), out_gain.reshape(1, H), tokens, w_gate, w_up, w_down)


def solution(mesh):
    placed = (
        P(("grp", "ep"), None),
        P(),
        P(("grp", "ep"), None),
        P(("grp", "ep"), None),
        P("ep", None, "tp"),
        P("ep", None, "tp"),
        P("ep", "tp", None),
        P("tp"),
    )
    return jax.shard_map(
        body, mesh=mesh, in_specs=placed, out_specs=P(("grp", "ep"), "tp"), check_vma=False
    )
```

profile of v0, /device:TPU:0, one launch (start us, length us, event | category | flops | bytes accessed | tf_op | source)
XLA Modules:
  0.0 47.3 jit_solution(13923770184906444856)
XLA Ops:
  0.0 45.7 %shard_map.82 = bf16[128,1024]{1,0:T(8,128)(2,1)} custom-call(s32[4,128]{1,0:T(4,128)} %bitcast.6, f32[4,128]{1,0:T(4,128)} %bitcast.7, f32[1,2048]{1,0:T(1,128)} %bitcast.4, f32[1,1024]{1,0:T(1,128)} %bitcast.5, bf16[128,2048]{1,0:T(8,128)(2,1)} %tokens_hbm.1, bf16[2,2048,256]{2,1,0:T(8,128)(2,1)} %gate_hbm.1, bf16[2,2048,256]{2,1,0:T(8,128)(2,1)} %up_hbm.1, ...), custom_call_target="tpu_custom_call" | custom-call | tf_op jit(solution)/shard_map/pallas_call | solution.py:310
  45.7 1.7 %copy.10 = bf16[128,1024]{1,0:T(8,128)(2,1)} copy(bf16[128,1024]{1,0:T(8,128)(2,1)} %shard_map.82) | data formatting | bytes 524288
where the time goes:
time: 47.5 us; the launch traced here: 47.3 us
  Pallas kernels  45.7 us (96%)
  local copies, waits for them, and re-layouts  1.67 us (4%)
    pallas_call x1, Pallas kernels, body(): pl.pallas_call(functools.partial(kernel, Q, S, R), out_shape=jax.ShapeDty...  45.7 us
    unnamed x1, local copies, waits for them, and re-layouts  1.67 us

commit v1 on v0

v1 whole, which is shorter than its diff:
```python
import functools

import jax
import jax.numpy as jnp
from jax import lax
from jax.experimental import pallas as pl
from jax.experimental.pallas import tpu as pltpu
from jax.sharding import PartitionSpec as P

GROUPS = 4
EPS = 1e-06
MESH = pl.DeviceIdType.MESH
F32 = jnp.float32
BF16 = jnp.bfloat16

STEPS = (
    "A11", "B01", "A10", "B00", "G01", "B11", "G00", "A21", "B10", "G11", "A20", "G10",
    "D11", "D10", "B21", "A31", "G21", "D01", "B20", "G20", "D00", "A30", "F11", "F10",
    "D21", "B31", "D20", "G31", "B30", "D31", "G30", "F21", "D30", "F20", "F01", "F00",
    "M01", "M00", "F31", "F30", "M11", "M10", "M21", "M20", "M31", "M30",
)


def loop(low, high, step):
    if high - low <= 8:
        for i in range(low, high):
            step(i)
    else:
        lax.fori_loop(low, high, lambda i, carry: (step(i), carry)[1], 0)


def partner(q, d, count):
    if count & (count - 1):
        return lax.rem(q + d, count), lax.rem(q + count - d, count)
    other, bit = 0, 1
    while bit < count:
        mine, theirs = (q // bit) % 2, (d // bit) % 2
        other = other + bit * (mine + theirs - 2 * mine * theirs)
        bit *= 2
    return other, other


def kernel(
    group_count, span, rows,
    routes_ref, probs_ref, in_gain_ref, out_gain_ref, tokens_hbm, gate_hbm, up_hbm, down_hbm,
    out_ref,
    tokens_ref, sendz, gathered, unpack, gate_send, gate_recv, w_gate, w_up, w_down, spare, hidden,
    r_send, own_sum, r_recv, home_send, home_recv, mixed, sq_send, sq_recv,
    tok_sem, w_sem, gate_ss, gate_rs, z_ss, z_rs, x_ss, x_rs, t_ss, t_rs, u_ss, u_rs, v_ss, v_rs,
    r_ss, r_rs, h_ss, h_rs, q_ss, q_rs,
):
    Q, S, R = group_count, span, rows
    N = Q * S
    RC = R // 2
    top, tok = routes_ref.shape
    width = tokens_ref.shape[1]
    H = out_ref.shape[1]
    L, _, F = gate_hbm.shape
    LF = L * F
    group_width = S * L
    lanes = gate_send.shape[-1]
    me = lax.axis_index("ep")
    c = lax.axis_index("tp")
    q, s = me // S, lax.rem(me, S)
    if Q == 4:
        middle = (q + 1) // 2 % 2
        place, order = [0, 3 - middle, 1, 2 + middle], [3 - 2 * middle, 2 + middle, 1 + middle]
    else:
        place, order = list(range(Q)), list(range(1, Q))
    pair = 2 if S % 2 == 0 else 1
    rows_at_once = pair * RC

    def at(ep, tp=None):
        return {"ep": ep, "tp": c if tp is None else tp}

    def remote(src, dst, ss, rs, dev):
        return pltpu.make_async_remote_copy(
            src_ref=src, dst_ref=dst, send_sem=ss, recv_sem=rs, device_id=dev, device_id_type=MESH
        )

    def chunk(k):
        return pl.ds(k * RC, RC)

    tok_copy = pltpu.make_async_copy(tokens_hbm, tokens_ref, tok_sem)
    tok_copy.start()

    barrier = pltpu.get_barrier_semaphore()
    loop(1, N, lambda p: pl.semaphore_signal(
        barrier, inc=1, device_id=at(lax.rem(me + p, N)), device_id_type=MESH))
    pl.semaphore_signal(barrier, inc=1, device_id=at(me, 1 - c), device_id_type=MESH)

    own_cols = pl.ds(pl.multiple_of(c * H, H), H)
    other_cols = pl.ds(pl.multiple_of((1 - c) * H, H), H)
    weights = []
    for n, (src, dst) in enumerate(((gate_hbm, w_gate), (up_hbm, w_up))):
        for e in range(L):
            weights.append(pltpu.make_async_copy(src.at[e], dst.at[e], w_sem.at[n, e]))
    for e in range(L):
        weights.append(pltpu.make_async_copy(
            down_hbm.at[e, :, own_cols], w_down.at[0, pl.ds(e * F, F)], w_sem.at[2, e]))
    away = [
        pltpu.make_async_copy(down_hbm.at[e, :, other_cols], spare.at[pl.ds(e * F, F)], w_sem.at[3, e]) for e in range(L)
    ]

    first = routes_ref[0:1, :]
    row_group = lax.broadcasted_iota(jnp.int32, (16, tok), 0)
    groups = jnp.full((16, tok), -1, jnp.int32)
    for d in range(Q):
        groups = jnp.where(row_group == d, partner(q, d, Q)[0], groups)
    member = (groups >= 0) & (first >= groups * group_width) & (first < (groups + 1) * group_width)
    earlier = lax.broadcasted_iota(jnp.int32, (tok, tok), 0) < lax.broadcasted_iota(jnp.int32, (tok, tok), 1)
    rank = jnp.dot(
        jnp.where(member, 1.0, 0.0).astype(BF16), jnp.where(earlier, 1.0, 0.0).astype(BF16),
        preferred_element_type=F32,
    ).astype(jnp.int32)
    slots = lax.broadcasted_iota(jnp.int32, (lanes, tok), 0)
    picks = []
    for d in range(Q):
        low = partner(q, d, Q)[0] * group_width
        inside = (first >= low) & (first < low + group_width)
        picks.append(jnp.where((rank[d:d + 1, :] == slots) & inside, 1.0, 0.0))

    tok_copy.wait()
    for copy in away + weights:
        copy.start()
    floats = tokens_ref[...].astype(F32)
    inv = lax.rsqrt(jnp.mean(floats * floats, axis=-1, keepdims=True) + EPS)
    normed = (tokens_ref[...].astype(F32) * inv * in_gain_ref[...]).astype(BF16)
    for d in range(Q):
        pick = jnp.where(c == 0, picks[d][:RC], picks[d][RC:R]).astype(BF16)
        block = jnp.dot(pick, normed, preferred_element_type=F32).astype(BF16)
        if d == 0:
            gathered[0, c, 0] = block
        else:
            sendz[d] = block

    pl.semaphore_wait(barrier, N)

    def z_copy(d):
        return remote(sendz.at[d], gathered.at[d, c, 0], z_ss.at[d], z_rs.at[d], at(partner(q, d, Q)[0] * S + s))

    def x_copy(d, e):
        return remote(
            gathered.at[d, c, 0], gathered.at[d, c, e], x_ss.at[d, e], x_rs.at[d, e], at(q * S + lax.rem(s + e, S)))

    def t_copy(d, e):
        block = gathered.at[d, c, e]
        return remote(block, block, t_ss.at[d, e], t_rs.at[d, e], at(me, 1 - c))

    def gate_copy(d, e):
        return remote(
            gate_send.at[d, lax.rem(s + e, S)], gate_recv.at[d, e], gate_ss.at[d, e], gate_rs.at[d, e],
            at(partner(q, d, Q)[0] * S + lax.rem(s + e, S)),
        )

    def u_copy():
        return remote(spare, w_down.at[1], u_ss, u_rs, at(me, 1 - c))

    def v_copy(d, k):
        return remote(hidden.at[d, k, 0], hidden.at[d, k, 1], v_ss.at[d, k], v_rs.at[d, k], at(me, 1 - c))

    def r_copy(d, e, k):
        return remote(
            r_send.at[d, k, e], r_recv.at[d, k, e], r_ss.at[d, e, k], r_rs.at[d, e, k],
            at(q * S + lax.rem(s + S - e, S)),
        )

    def h_copy(d, k):
        return remote(
            home_send.at[d, k], home_recv.at[d, k], h_ss.at[d, k], h_rs.at[d, k], at(partner(q, d, Q)[1] * S + s))

    def forward(d):
        loop(1, S, lambda e: x_copy(d, e).start())
        t_copy(d, 0).start()

    forward(0)
    for d in order:
        z_copy(d).start()
    for copy in away:
        copy.wait()
    u_copy().start()

    for d in range(Q):
        base = partner(q, d, Q)[0] * group_width
        ids = base + lax.broadcasted_iota(jnp.int32, (-(-group_width // 8) * 8, tok), 0)
        dense = jnp.zeros(ids.shape, F32)
        for k in range(top):
            dense += jnp.where(routes_ref[k:k + 1, :] == ids, probs_ref[k:k + 1, :], 0.0)
        lines = lax.dot_general(
            dense, picks[d], (((1,), (1,)), ((), ())),
            precision=lax.Precision.HIGHEST, preferred_element_type=F32,
        )
        for i in range(S):
            gate_send[d, i] = lines[i * L:(i + 1) * L]
    gate_recv[0, 0] = gate_send[0, s]
    for d in range(Q):
        loop(1 if d == 0 else 0, S, lambda e: gate_copy(d, e).start())

    for d in range(Q):
        for k in range(2):
            unpack[d, k] = picks[d][k * RC:(k + 1) * RC].T.astype(BF16)
    for copy in weights:
        copy.wait()

    row, lane = (lax.broadcasted_iota(jnp.int32, (RC, lanes), i) for i in (0, 1))

    def up_projection(d, k, n):
        base = n * pair
        tokens = gathered[d, k, pl.ds(base, pair)].reshape(rows_at_once, width)
        at_rows = pl.ds(n * rows_at_once, rows_at_once)
        for j in range(L):
            gate = jnp.dot(tokens, w_gate[j], preferred_element_type=F32)
            up = jnp.dot(tokens, w_up[j], preferred_element_type=F32)
            scale = jnp.concatenate([
                jnp.sum(jnp.where(row + k * RC == lane, gate_recv[d, base + b, pl.ds(j, 1), :], 0.0), axis=1, keepdims=True)
                for b in range(pair)
            ], axis=0)
            act = gate / (1.0 + jnp.exp(-gate)) * up
            hidden[d, k, 0, at_rows, j * F:(j + 1) * F] = (act * scale).astype(BF16)

    def down_projection(d, k, n, ready):
        at_rows = pl.ds(n * rows_at_once, rows_at_once)
        part = jnp.dot(hidden[d, k, 0, at_rows], w_down[0], preferred_element_type=F32)
        ready()
        return part + jnp.dot(hidden[d, k, 1, at_rows], w_down[1], preferred_element_type=F32)

    down_ready = []

    def step_a(p, k):
        d = place[p]

        @pl.when(c == k)
        def _():
            z_copy(d).wait_recv()
            forward(d)

    def step_b(p, k):
        d = place[p]

        def one(e):
            x_copy(d, e).wait_recv()
            t_copy(d, e).start()
        pl.when(c == k)(lambda: loop(1, S, one))

    def step_g(p, k):
        d = place[p]
        if k == 1:
            loop(1 if p == 0 else 0, S, lambda e: gate_copy(d, e).wait_recv())
        pl.when(c != k)(lambda: loop(0, S, lambda e: t_copy(d, e).wait_recv()))
        if S == pair:
            up_projection(d, k, 0)
        else:
            lax.fori_loop(0, S // pair, lambda n, carry: (up_projection(d, k, n), carry)[1], 0)
        v_copy(d, k).start()

    def step_d(p, k):
        d = place[p]
        if not down_ready:
            u_copy().wait_recv()
            down_ready.append(True)
        out = down_projection(d, k, 0, v_copy(d, k).wait_recv)
        for e in range(1, pair):
            r_send[d, k, e] = out[e * RC:(e + 1) * RC].astype(BF16)
        own_sum[d, k] = out[:RC]
        if S > pair:
            def some(n, carry):
                out = down_projection(d, k, n, lambda: None)
                r_send[d, k, pl.ds(n * pair, pair)] = out.astype(BF16).reshape(pair, RC, H)
                return carry
            lax.fori_loop(1, S // pair, some, 0)
        loop(1, S, lambda e: r_copy(d, e, k).start())

    def step_f(p, k):
        d = place[p]

        def one(e, total):
            r_copy(d, e, k).wait_recv()
            return total + r_recv[d, k, e].astype(F32)
        total = own_sum[d, k]
        if S <= 8:
            for e in range(1, S):
                total = one(e, total)
        else:
            total = lax.fori_loop(1, S, one, total)
        if p == 0:
            home_recv[0, k] = total.astype(BF16)
        else:
            home_send[d, k] = total.astype(BF16)
            h_copy(d, k).start()

    def step_m(p, k):
        d = place[p]
        if p > 0:
            h_copy(d, k).wait_recv()
        term = jnp.dot(unpack[d, k], home_recv[d, k], preferred_element_type=F32)
        mixed[...] = term if (p, k) == (0, 1) else mixed[...] + term

    actions = {"A": step_a, "B": step_b, "G": step_g, "D": step_d, "F": step_f, "M": step_m}

    steps = STEPS
    if Q != 4:
        units = [f"{p}{k}" for p in range(Q) for k in (1, 0)]
        steps = ["A" + u for u in units[2:]] + [x + u for x in "BGDFM" for u in units]
    for step in steps:
        actions[step[0]](*(int(i) for i in step[1:]))

    total = mixed[...]
    squares = jnp.sum(total * total, axis=1, keepdims=True)
    sq_send[...] = jnp.broadcast_to(squares, sq_send.shape)
    sq_copy = remote(sq_send, sq_recv, q_ss, q_rs, at(me, 1 - c))
    sq_copy.start()
    u_copy().wait_send()
    for d in range(Q):
        loop(1 if d == 0 else 0, S, lambda e: gate_copy(d, e).wait_send())
        loop(0, S, lambda e: t_copy(d, e).wait_send())
        loop(1, S, lambda e: x_copy(d, e).wait_send())
        if d > 0:
            z_copy(d).wait_send()
        for k in range(2):
            v_copy(d, k).wait_send()
            if d > 0:
                h_copy(d, k).wait_send()
            loop(1, S, lambda e: r_copy(d, e, k).wait_send())
    sq_copy.wait()
    norm = lax.rsqrt((squares + sq_recv[:, 0:1]) / width + EPS)
    out_ref[...] = (total * norm * out_gain_ref[...]).astype(BF16)


def body(tokens, in_gain, routing, gate_prob, w_gate, w_up, w_down, out_gain):
    N = lax.axis_size("ep")
    L, D, F = w_gate.shape
    tok, top = routing.shape
    H = out_gain.shape[0]
    group_width = L * N // GROUPS
    cap = max(2, tok * top // (2 * group_width))
    R = min(tok, group_width * cap // top)
    R = -(-R // 16) * 16
    Q, S, K = GROUPS, N // GROUPS, 2
    RC = R // K
    lanes = -(-R // 128) * 128
    vmem = pl.BlockSpec(memory_space=pltpu.VMEM)
    hbm = pl.BlockSpec(memory_space=pl.ANY)
    dma = pltpu.SemaphoreType.DMA
    return pl.pallas_call(
        functools.partial(kernel, Q, S, R),
        out_shape=jax.ShapeDtypeStruct((tok, H), BF16),
        in_specs=[vmem] * 4 + [hbm] * 4,
        out_specs=vmem,
        scratch_shapes=[
            pltpu.VMEM((tok, D), BF16),
            pltpu.VMEM((Q, RC, D), BF16),
            pltpu.VMEM((Q, K, S, RC, D), BF16),
            pltpu.VMEM((Q, K, tok, RC), BF16),
            pltpu.VMEM((Q, S, L, lanes), F32),
            pltpu.VMEM((Q, S, L, lanes), F32),
            pltpu.VMEM((L, D, F), BF16),
            pltpu.VMEM((L, D, F), BF16),
            pltpu.VMEM((2, L * F, H), BF16),
            pltpu.VMEM((L * F, H), BF16),
            pltpu.VMEM((Q, K, 2, S * RC, L * F), BF16),
            pltpu.VMEM((Q, K, S, RC, H), BF16),
            pltpu.VMEM((Q, K, RC, H), F32),
            pltpu.VMEM((Q, K, S, RC, H), BF16),
            pltpu.VMEM((Q, K, RC, H), BF16),
            pltpu.VMEM((Q, K, RC, H), BF16),
            pltpu.VMEM((tok, H), F32),
            pltpu.VMEM((tok, 128), F32),
            pltpu.VMEM((tok, 128), F32),
            dma, dma((4, L)), dma((Q, S)), dma((Q, S)), dma((Q,)), dma((Q,)),
            dma((Q, S)), dma((Q, S)), dma((Q, S)), dma((Q, S)), dma, dma,
            dma((Q, K)), dma((Q, K)), dma((Q, S, K)), dma((Q, S, K)), dma((Q, K)), dma((Q, K)),
            dma, dma,
        ],
        compiler_params=pltpu.CompilerParams(
            collective_id=0, has_side_effects=True, vmem_limit_bytes=64 * 1000 * 1000
        ),
    )(routing.T, gate_prob.T, in_gain.reshape(1, D), out_gain.reshape(1, H), tokens, w_gate, w_up, w_down)


def solution(mesh):
    placed = (
        P(("grp", "ep"), None),
        P(),
        P(("grp", "ep"), None),
        P(("grp", "ep"), None),
        P("ep", None, "tp"),
        P("ep", None, "tp"),
        P("ep", "tp", None),
        P("tp"),
    )
    return jax.shard_map(
        body, mesh=mesh, in_specs=placed, out_specs=P(("grp", "ep"), "tp"), check_vma=False
    )
```

time: 47.5 us -> 47.7 us (level)
  the two profiles are of different devices: /device:TPU:0 before, /device:TPU:13 now
where the time goes in v1:
time: 47.7 us; the launch traced here: 47.4 us
  Pallas kernels  45.8 us (96%)
  local copies, waits for them, and re-layouts  1.67 us (4%)
    pallas_call x1, Pallas kernels, body(): pl.pallas_call(functools.partial(kernel, Q, S, R), out_shape=jax.ShapeDty...  45.8 us
    unnamed x1, local copies, waits for them, and re-layouts  1.67 us

profile of v1, /device:TPU:13, one launch (start us, length us, event | category | flops | bytes accessed | tf_op | source)
XLA Modules:
  0.0 47.4 jit_solution(7336708529967815538)
XLA Ops:
  0.0 45.8 %shard_map.82 = bf16[128,1024]{1,0:T(8,128)(2,1)} custom-call(s32[4,128]{1,0:T(4,128)} %bitcast.6, f32[4,128]{1,0:T(4,128)} %bitcast.7, f32[1,2048]{1,0:T(1,128)} %bitcast.4, f32[1,1024]{1,0:T(1,128)} %bitcast.5, bf16[128,2048]{1,0:T(8,128)(2,1)} %tokens_hbm.1, bf16[2,2048,256]{2,1,0:T(8,128)(2,1)} %gate_hbm.1, bf16[2,2048,256]{2,1,0:T(8,128)(2,1)} %up_hbm.1, ...), custom_call_target="tpu_custom_call" | custom-call | tf_op jit(solution)/shard_map/pallas_call | solution.py:344
  45.8 1.7 %copy.10 = bf16[128,1024]{1,0:T(8,128)(2,1)} copy(bf16[128,1024]{1,0:T(8,128)(2,1)} %shard_map.82) | data formatting | bytes 524288

commit v2 on v1

--- a/solution.py
+++ b/solution.py
@@ -14,11 +14,14 @@
 BF16 = jnp.bfloat16
 
 STEPS = (
-    "A11", "B01", "A10", "B00", "G01", "B11", "G00", "A21", "B10", "G11", "A20", "G10",
-    "D11", "D10", "B21", "A31", "G21", "D01", "B20", "G20", "D00", "A30", "F11", "F10",
-    "D21", "B31", "D20", "G31", "B30", "D31", "G30", "F21", "D30", "F20", "F01", "F00",
-    "M01", "M00", "F31", "F30", "M11", "M10", "M21", "M20", "M31", "M30",
+    "A21", "A11", "A20", "A10", "B21", "G21", "B01", "B11", "A31", "D21", "B20", "G20",
+    "B10", "B00", "A30", "G11", "B31", "D20", "D11", "F21", "G31", "G10", "B30", "D31",
+    "F20", "G30", "F11", "D30", "G00", "F31", "D10", "D00", "G01", "F30", "D01", "F10",
+    "M21", "M31", "M11", "F00", "M00", "M20", "F01", "M01", "M10", "M30",
 )
+PLACES = ((1, 2, 3), (2, 1, 3), (1, 2, 3), (1, 2, 3))
+ORDERS = ((1, 2, 3), (2, 3, 1), (1, 2, 3), (1, 2, 3))
+PARTS = 2
 
 
 def loop(low, high, step):
@@ -42,9 +45,9 @@
 
 def kernel(
     group_count, span, rows,
-    routes_ref, probs_ref, in_gain_ref, out_gain_ref, tokens_hbm, gate_hbm, up_hbm, down_hbm,
+    routes_hbm, probs_hbm, in_gain_hbm, out_gain_hbm, tokens_hbm, gate_hbm, up_hbm, down_hbm,
     out_ref,
-    tokens_ref, sendz, gathered, unpack, gate_send, gate_recv, w_gate, w_up, w_down, spare, hidden,
+    routes_ref, probs_ref, in_gain_ref, out_gain_ref, tokens_ref, sendz, gathered, unpack, gate_send, gate_recv, w_gate, w_up, w_down, spare, hidden,
     r_send, own_sum, r_recv, home_send, home_recv, mixed, sq_send, sq_recv,
     tok_sem, w_sem, gate_ss, gate_rs, z_ss, z_rs, x_ss, x_rs, t_ss, t_rs, u_ss, u_rs, v_ss, v_rs,
     r_ss, r_rs, h_ss, h_rs, q_ss, q_rs,
@@ -56,15 +59,18 @@
     width = tokens_ref.shape[1]
     H = out_ref.shape[1]
     L, _, F = gate_hbm.shape
-    LF = L * F
+    W = width // PARTS
     group_width = S * L
     lanes = gate_send.shape[-1]
     me = lax.axis_index("ep")
     c = lax.axis_index("tp")
     q, s = me // S, lax.rem(me, S)
     if Q == 4:
-        middle = (q + 1) // 2 % 2
-        place, order = [0, 3 - middle, 1, 2 + middle], [3 - 2 * middle, 2 + middle, 1 + middle]
+        digit = (1 + 3 * (q % 2)) * (1 + 15 * (q // 2))
+
+        def look_up(table):
+            return [sum(row[i] * 4 ** z for z, row in enumerate(table)) // digit % 4 for i in range(3)]
+        place, order = [0] + look_up(PLACES), look_up(ORDERS)
     else:
         place, order = list(range(Q)), list(range(1, Q))
     pair = 2 if S % 2 == 0 else 1
@@ -81,8 +87,15 @@
     def chunk(k):
         return pl.ds(k * RC, RC)
 
-    tok_copy = pltpu.make_async_copy(tokens_hbm, tokens_ref, tok_sem)
+    small = [
+        pltpu.make_async_copy(src, dst, tok_sem.at[i]) for i, (src, dst) in enumerate((
+            (routes_hbm, routes_ref), (in_gain_hbm, in_gain_ref), (probs_hbm, probs_ref), (out_gain_hbm, out_gain_ref)))
+    ]
+    tok_copy = pltpu.make_async_copy(tokens_hbm, tokens_ref, tok_sem.at[4])
+    small[0].start()
     tok_copy.start()
+    for copy in small[1:]:
+        copy.start()
 
     barrier = pltpu.get_barrier_semaphore()
     loop(1, N, lambda p: pl.semaphore_signal(
@@ -102,6 +115,7 @@
         pltpu.make_async_copy(down_hbm.at[e, :, other_cols], spare.at[pl.ds(e * F, F)], w_sem.at[3, e]) for e in range(L)
     ]
 
+    small[0].wait()
     first = routes_ref[0:1, :]
     row_group = lax.broadcasted_iota(jnp.int32, (16, tok), 0)
     groups = jnp.full((16, tok), -1, jnp.int32)
@@ -121,6 +135,7 @@
         picks.append(jnp.where((rank[d:d + 1, :] == slots) & inside, 1.0, 0.0))
 
     tok_copy.wait()
+    small[1].wait()
     for copy in away + weights:
         copy.start()
     floats = tokens_ref[...].astype(F32)
@@ -129,23 +144,27 @@
     for d in range(Q):
         pick = jnp.where(c == 0, picks[d][:RC], picks[d][RC:R]).astype(BF16)
         block = jnp.dot(pick, normed, preferred_element_type=F32).astype(BF16)
-        if d == 0:
-            gathered[0, c, 0] = block
-        else:
-            sendz[d] = block
+        for h in range(PARTS):
+            if d == 0:
+                gathered[0, c, h, 0] = block[:, h * W:(h + 1) * W]
+            else:
+                sendz[d, h] = block[:, h * W:(h + 1) * W]
 
     pl.semaphore_wait(barrier, N)
 
-    def z_copy(d):
-        return remote(sendz.at[d], gathered.at[d, c, 0], z_ss.at[d], z_rs.at[d], at(partner(q, d, Q)[0] * S + s))
-
-    def x_copy(d, e):
+    def z_copy(d, h):
         return remote(
-            gathered.at[d, c, 0], gathered.at[d, c, e], x_ss.at[d, e], x_rs.at[d, e], at(q * S + lax.rem(s + e, S)))
-
-    def t_copy(d, e):
-        block = gathered.at[d, c, e]
-        return remote(block, block, t_ss.at[d, e], t_rs.at[d, e], at(me, 1 - c))
+            sendz.at[d, h], gathered.at[d, c, h, 0], z_ss.at[d, h], z_rs.at[d, h], at(partner(q, d, Q)[0] * S + s))
+
+    def x_copy(d, e, h):
+        return remote(
+            gathered.at[d, c, h, 0], gathered.at[d, c, h, e], x_ss.at[d, e, h], x_rs.at[d, e, h],
+            at(q * S + lax.rem(s + e, S)),
+        )
+
+    def t_copy(d, e, h):
+        block = gathered.at[d, c, h, e]
+        return remote(block, block, t_ss.at[d, e, h], t_rs.at[d, e, h], at(me, 1 - c))
 
     def gate_copy(d, e):
         return remote(
@@ -169,17 +188,21 @@
         return remote(
             home_send.at[d, k], home_recv.at[d, k], h_ss.at[d, k], h_rs.at[d, k], at(partner(q, d, Q)[1] * S + s))
 
-    def forward(d):
-        loop(1, S, lambda e: x_copy(d, e).start())
-        t_copy(d, 0).start()
-
-    forward(0)
+    def forward(d, h):
+        loop(1, S, lambda e: x_copy(d, e, h).start())
+        t_copy(d, 0, h).start()
+
+    for h in range(PARTS):
+        forward(0, h)
     for d in order:
-        z_copy(d).start()
+        for h in range(PARTS):
+            z_copy(d, h).start()
     for copy in away:
         copy.wait()
     u_copy().start()
 
+    small[2].wait()
+    small[3].wait()
     for d in range(Q):
         base = partner(q, d, Q)[0] * group_width
         ids = base + lax.broadcasted_iota(jnp.int32, (-(-group_width // 8) * 8, tok), 0)
@@ -206,7 +229,8 @@
 
     def up_projection(d, k, n):
         base = n * pair
-        tokens = gathered[d, k, pl.ds(base, pair)].reshape(rows_at_once, width)
+        tokens = jnp.concatenate(
+            [gathered[d, k, h, pl.ds(base, pair)].reshape(rows_at_once, W) for h in range(PARTS)], axis=1)
         at_rows = pl.ds(n * rows_at_once, rows_at_once)
         for j in range(L):
             gate = jnp.dot(tokens, w_gate[j], preferred_element_type=F32)
@@ -224,29 +248,37 @@
         ready()
         return part + jnp.dot(hidden[d, k, 1, at_rows], w_down[1], preferred_element_type=F32)
 
-    down_ready = []
+    down_ready, gates_ready, mixed_ready = [], [], []
 
     def step_a(p, k):
         d = place[p]
 
         @pl.when(c == k)
         def _():
-            z_copy(d).wait_recv()
-            forward(d)
+            for h in range(PARTS):
+                z_copy(d, h).wait_recv()
+                forward(d, h)
 
     def step_b(p, k):
         d = place[p]
 
         def one(e):
-            x_copy(d, e).wait_recv()
-            t_copy(d, e).start()
+            for h in range(PARTS):
+                x_copy(d, e, h).wait_recv()
+                t_copy(d, e, h).start()
         pl.when(c == k)(lambda: loop(1, S, one))
 
     def step_g(p, k):
         d = place[p]
-        if k == 1:
+        if p not in gates_ready:
             loop(1 if p == 0 else 0, S, lambda e: gate_copy(d, e).wait_recv())
-        pl.when(c != k)(lambda: loop(0, S, lambda e: t_copy(d, e).wait_recv()))
+            gates_ready.append(p)
+
+
+        def arrived(e):
+            for h in range(PARTS):
+                t_copy(d, e, h).wait_recv()
+        pl.when(c != k)(lambda: loop(0, S, arrived))
         if S == pair:
             up_projection(d, k, 0)
         else:
@@ -293,7 +325,8 @@
         if p > 0:
             h_copy(d, k).wait_recv()
         term = jnp.dot(unpack[d, k], home_recv[d, k], preferred_element_type=F32)
-        mixed[...] = term if (p, k) == (0, 1) else mixed[...] + term
+        mixed[...] = mixed[...] + term if mixed_ready else term
+        mixed_ready.append(True)
 
     actions = {"A": step_a, "B": step_b, "G": step_g, "D": step_d, "F": step_f, "M": step_m}
 
@@ -312,10 +345,11 @@
     u_copy().wait_send()
     for d in range(Q):
         loop(1 if d == 0 else 0, S, lambda e: gate_copy(d, e).wait_send())
-        loop(0, S, lambda e: t_copy(d, e).wait_send())
-        loop(1, S, lambda e: x_copy(d, e).wait_send())
-        if d > 0:
-            z_copy(d).wait_send()
+        for h in range(PARTS):
+            loop(0, S, lambda e: t_copy(d, e, h).wait_send())
+            loop(1, S, lambda e: x_copy(d, e, h).wait_send())
+            if d > 0:
+                z_copy(d, h).wait_send()
         for k in range(2):
             v_copy(d, k).wait_send()
             if d > 0:
@@ -344,12 +378,16 @@
     return pl.pallas_call(
         functools.partial(kernel, Q, S, R),
         out_shape=jax.ShapeDtypeStruct((tok, H), BF16),
-        in_specs=[vmem] * 4 + [hbm] * 4,
+        in_specs=[hbm] * 8,
         out_specs=vmem,
         scratch_shapes=[
+            pltpu.VMEM((top, tok), jnp.int32),
+            pltpu.VMEM((top, tok), F32),
+            pltpu.VMEM((1, D), F32),
+            pltpu.VMEM((1, H), F32),
             pltpu.VMEM((tok, D), BF16),
-            pltpu.VMEM((Q, RC, D), BF16),
-            pltpu.VMEM((Q, K, S, RC, D), BF16),
+            pltpu.VMEM((Q, PARTS, RC, D // PARTS), BF16),
+            pltpu.VMEM((Q, K, PARTS, S, RC, D // PARTS), BF16),
             pltpu.VMEM((Q, K, tok, RC), BF16),
             pltpu.VMEM((Q, S, L, lanes), F32),
             pltpu.VMEM((Q, S, L, lanes), F32),
@@ -366,8 +404,8 @@
             pltpu.VMEM((tok, H), F32),
             pltpu.VMEM((tok, 128), F32),
             pltpu.VMEM((tok, 128), F32),
-            dma, dma((4, L)), dma((Q, S)), dma((Q, S)), dma((Q,)), dma((Q,)),
-            dma((Q, S)), dma((Q, S)), dma((Q, S)), dma((Q, S)), dma, dma,
+            dma((5,)), dma((4, L)), dma((Q, S)), dma((Q, S)), dma((Q, PARTS)), dma((Q, PARTS)),
+            dma((Q, S, PARTS)), dma((Q, S, PARTS)), dma((Q, S, PARTS)), dma((Q, S, PARTS)), dma, dma,
             dma((Q, K)), dma((Q, K)), dma((Q, S, K)), dma((Q, S, K)), dma((Q, K)), dma((Q, K)),
             dma, dma,
         ],

time: 47.7 us -> 44.4 us (0.931)
  the two profiles are of different devices: /device:TPU:13 before, /device:TPU:0 now
where the time goes in v2:
time: 44.4 us; the launch traced here: 44.2 us
  Pallas kernels  42.5 us (96%)
  local copies, waits for them, and re-layouts  1.67 us (4%)
    pallas_call x1, Pallas kernels, body(): pl.pallas_call(functools.partial(kernel, Q, S, R), out_shape=jax.ShapeDty...  42.5 us
    unnamed x1, local copies, waits for them, and re-layouts  1.67 us

profile of v2, /device:TPU:0, one launch (start us, length us, event | category | flops | bytes accessed | tf_op | source)
XLA Modules:
  0.0 44.2 jit_solution(18032262731289317951)
XLA Ops:
  0.0 42.5 %shard_map.82 = bf16[128,1024]{1,0:T(8,128)(2,1)} custom-call(s32[4,128]{1,0:T(4,128)} %bitcast.6, f32[4,128]{1,0:T(4,128)} %bitcast.7, f32[1,2048]{1,0:T(1,128)} %bitcast.4, f32[1,1024]{1,0:T(1,128)} %bitcast.5, bf16[128,2048]{1,0:T(8,128)(2,1)} %tokens_hbm.1, bf16[2,2048,256]{2,1,0:T(8,128)(2,1)} %gate_hbm.1, bf16[2,2048,256]{2,1,0:T(8,128)(2,1)} %up_hbm.1, ...), custom_call_target="tpu_custom_call" | custom-call | tf_op jit(solution)/shard_map/pallas_call | solution.py:378
  42.5 1.7 %copy.10 = bf16[128,1024]{1,0:T(8,128)(2,1)} copy(bf16[128,1024]{1,0:T(8,128)(2,1)} %shard_map.82) | data formatting | bytes 524288

commit v3 on v2

--- a/solution.py
+++ b/solution.py
@@ -14,13 +14,13 @@
 BF16 = jnp.bfloat16
 
 STEPS = (
-    "A21", "A11", "A20", "A10", "B21", "G21", "B01", "B11", "A31", "D21", "B20", "G20",
-    "B10", "B00", "A30", "G11", "B31", "D20", "D11", "F21", "G31", "G10", "B30", "D31",
-    "F20", "G30", "F11", "D30", "G00", "F31", "D10", "D00", "G01", "F30", "D01", "F10",
-    "M21", "M31", "M11", "F00", "M00", "M20", "F01", "M01", "M10", "M30",
+    "B00", "A11", "A31", "B11", "G00", "B01", "A10", "A30", "G11", "A21", "B10", "D11",
+    "G10", "B30", "D10", "B31", "A20", "B21", "G30", "F11", "G21", "D30", "D21", "G31",
+    "B20", "F10", "D31", "G20", "F30", "D20", "F21", "G01", "F31", "D00", "D01", "F20",
+    "M10", "M30", "M21", "F00", "M00", "M11", "F01", "M01", "M20", "M31",
 )
-PLACES = ((1, 2, 3), (2, 1, 3), (1, 2, 3), (1, 2, 3))
-ORDERS = ((1, 2, 3), (2, 3, 1), (1, 2, 3), (1, 2, 3))
+PLACES = ((3, 2, 1), (2, 3, 1), (2, 3, 1), (3, 2, 1))
+ORDERS = ((3, 2, 1), (2, 1, 3), (2, 3, 1), (3, 2, 1))
 PARTS = 2
 
 
@@ -104,16 +104,12 @@
 
     own_cols = pl.ds(pl.multiple_of(c * H, H), H)
     other_cols = pl.ds(pl.multiple_of((1 - c) * H, H), H)
-    weights = []
-    for n, (src, dst) in enumerate(((gate_hbm, w_gate), (up_hbm, w_up))):
-        for e in range(L):
-            weights.append(pltpu.make_async_copy(src.at[e], dst.at[e], w_sem.at[n, e]))
-    for e in range(L):
-        weights.append(pltpu.make_async_copy(
-            down_hbm.at[e, :, own_cols], w_down.at[0, pl.ds(e * F, F)], w_sem.at[2, e]))
-    away = [
-        pltpu.make_async_copy(down_hbm.at[e, :, other_cols], spare.at[pl.ds(e * F, F)], w_sem.at[3, e]) for e in range(L)
+    weights = [
+        pltpu.make_async_copy(gate_hbm, w_gate, w_sem.at[0]),
+        pltpu.make_async_copy(up_hbm, w_up, w_sem.at[1]),
+        pltpu.make_async_copy(down_hbm.at[:, :, own_cols], w_down.at[0], w_sem.at[2]),
     ]
+    away = pltpu.make_async_copy(down_hbm.at[:, :, other_cols], spare, w_sem.at[3])
 
     small[0].wait()
     first = routes_ref[0:1, :]
@@ -136,7 +132,7 @@
 
     tok_copy.wait()
     small[1].wait()
-    for copy in away + weights:
+    for copy in [away] + weights:
         copy.start()
     floats = tokens_ref[...].astype(F32)
     inv = lax.rsqrt(jnp.mean(floats * floats, axis=-1, keepdims=True) + EPS)
@@ -148,27 +144,27 @@
             if d == 0:
                 gathered[0, c, h, 0] = block[:, h * W:(h + 1) * W]
             else:
-                sendz[d, h] = block[:, h * W:(h + 1) * W]
+                sendz[d - 1, h] = block[:, h * W:(h + 1) * W]
 
     pl.semaphore_wait(barrier, N)
 
     def z_copy(d, h):
         return remote(
-            sendz.at[d, h], gathered.at[d, c, h, 0], z_ss.at[d, h], z_rs.at[d, h], at(partner(q, d, Q)[0] * S + s))
+            sendz.at[d - 1, h], gathered.at[d, c, h, 0], z_ss, z_rs.at[d - 1, h], at(partner(q, d, Q)[0] * S + s))
 
     def x_copy(d, e, h):
         return remote(
-            gathered.at[d, c, h, 0], gathered.at[d, c, h, e], x_ss.at[d, e, h], x_rs.at[d, e, h],
+            gathered.at[d, c, h, 0], gathered.at[d, c, h, e], x_ss, x_rs.at[d, e - 1, h],
             at(q * S + lax.rem(s + e, S)),
         )
 
     def t_copy(d, e, h):
         block = gathered.at[d, c, h, e]
-        return remote(block, block, t_ss.at[d, e, h], t_rs.at[d, e, h], at(me, 1 - c))
-
-    def gate_copy(d, e):
+        return remote(block, block, t_ss, t_rs.at[d], at(me, 1 - c))
+
+    def gate_copy(d, e, near):
         return remote(
-            gate_send.at[d, lax.rem(s + e, S)], gate_recv.at[d, e], gate_ss.at[d, e], gate_rs.at[d, e],
+            gate_send.at[d, lax.rem(s + e, S)], gate_recv.at[d, e], gate_ss.at[near], gate_rs.at[d],
             at(partner(q, d, Q)[0] * S + lax.rem(s + e, S)),
         )
 
@@ -176,17 +172,17 @@
         return remote(spare, w_down.at[1], u_ss, u_rs, at(me, 1 - c))
 
     def v_copy(d, k):
-        return remote(hidden.at[d, k, 0], hidden.at[d, k, 1], v_ss.at[d, k], v_rs.at[d, k], at(me, 1 - c))
+        return remote(hidden.at[d, k, 0], hidden.at[d, k, 1], v_ss, v_rs.at[d, k], at(me, 1 - c))
 
     def r_copy(d, e, k):
         return remote(
-            r_send.at[d, k, e], r_recv.at[d, k, e], r_ss.at[d, e, k], r_rs.at[d, e, k],
+            r_send.at[d, k, e - 1], r_recv.at[d, k, e - 1], r_ss, r_rs.at[d, k],
             at(q * S + lax.rem(s + S - e, S)),
         )
 
     def h_copy(d, k):
         return remote(
-            home_send.at[d, k], home_recv.at[d, k], h_ss.at[d, k], h_rs.at[d, k], at(partner(q, d, Q)[1] * S + s))
+            home_send.at[d - 1, k], home_recv.at[d, k], h_ss, h_rs.at[d - 1, k], at(partner(q, d, Q)[1] * S + s))
 
     def forward(d, h):
         loop(1, S, lambda e: x_copy(d, e, h).start())
@@ -197,8 +193,7 @@
     for d in order:
         for h in range(PARTS):
             z_copy(d, h).start()
-    for copy in away:
-        copy.wait()
+    away.wait()
     u_copy().start()
 
     small[2].wait()
@@ -217,7 +212,7 @@
             gate_send[d, i] = lines[i * L:(i + 1) * L]
     gate_recv[0, 0] = gate_send[0, s]
     for d in range(Q):
-        loop(1 if d == 0 else 0, S, lambda e: gate_copy(d, e).start())
+        loop(1 if d == 0 else 0, S, lambda e: gate_copy(d, e, int(d == 0)).start())
 
     for d in range(Q):
         for k in range(2):
@@ -244,9 +239,15 @@
 
     def down_projection(d, k, n, ready):
         at_rows = pl.ds(n * rows_at_once, rows_at_once)
-        part = jnp.dot(hidden[d, k, 0, at_rows], w_down[0], preferred_element_type=F32)
+        part = jnp.dot(hidden[d, k, 0, at_rows], w_down[0].reshape(L * F, H), preferred_element_type=F32)
         ready()
-        return part + jnp.dot(hidden[d, k, 1, at_rows], w_down[1], preferred_element_type=F32)
+        return part + jnp.dot(hidden[d, k, 1, at_rows], w_down[1].reshape(L * F, H), preferred_element_type=F32)
+
+    def arrived(block, sem):
+        remote(block, block, sem, sem, at(me, 1 - c)).wait_recv()
+
+    def sent(block, sem):
+        remote(block, block, sem, sem, at(me, 1 - c)).wait_send()
 
     down_ready, gates_ready, mixed_ready = [], [], []
 
@@ -271,14 +272,10 @@
     def step_g(p, k):
         d = place[p]
         if p not in gates_ready:
-            loop(1 if p == 0 else 0, S, lambda e: gate_copy(d, e).wait_recv())
+            arrived(gate_recv.at[d, pl.ds(1, S - 1)] if p == 0 else gate_recv.at[d], gate_rs.at[d])
             gates_ready.append(p)
 
-
-        def arrived(e):
-            for h in range(PARTS):
-                t_copy(d, e, h).wait_recv()
-        pl.when(c != k)(lambda: loop(0, S, arrived))
+        pl.when(c != k)(lambda: arrived(gathered.at[d, 1 - c], t_rs.at[d]))
         if S == pair:
             up_projection(d, k, 0)
         else:
@@ -292,12 +289,12 @@
             down_ready.append(True)
         out = down_projection(d, k, 0, v_copy(d, k).wait_recv)
         for e in range(1, pair):
-            r_send[d, k, e] = out[e * RC:(e + 1) * RC].astype(BF16)
+            r_send[d, k, e - 1] = out[e * RC:(e + 1) * RC].astype(BF16)
         own_sum[d, k] = out[:RC]
         if S > pair:
             def some(n, carry):
                 out = down_projection(d, k, n, lambda: None)
-                r_send[d, k, pl.ds(n * pair, pair)] = out.astype(BF16).reshape(pair, RC, H)
+                r_send[d, k, pl.ds(n * pair - 1, pair)] = out.astype(BF16).reshape(pair, RC, H)
                 return carry
             lax.fori_loop(1, S // pair, some, 0)
         loop(1, S, lambda e: r_copy(d, e, k).start())
@@ -305,19 +302,17 @@
     def step_f(p, k):
         d = place[p]
 
-        def one(e, total):
-            r_copy(d, e, k).wait_recv()
-            return total + r_recv[d, k, e].astype(F32)
+        arrived(r_recv.at[d, k], r_rs.at[d, k])
         total = own_sum[d, k]
         if S <= 8:
             for e in range(1, S):
-                total = one(e, total)
+                total = total + r_recv[d, k, e - 1].astype(F32)
         else:
-            total = lax.fori_loop(1, S, one, total)
+            total = lax.fori_loop(1, S, lambda e, total: total + r_recv[d, k, e - 1].astype(F32), total)
         if p == 0:
             home_recv[0, k] = total.astype(BF16)
         else:
-            home_send[d, k] = total.astype(BF16)
+            home_send[d - 1, k] = total.astype(BF16)
             h_copy(d, k).start()
 
     def step_m(p, k):
@@ -343,18 +338,14 @@
     sq_copy = remote(sq_send, sq_recv, q_ss, q_rs, at(me, 1 - c))
     sq_copy.start()
     u_copy().wait_send()
-    for d in range(Q):
-        loop(1 if d == 0 else 0, S, lambda e: gate_copy(d, e).wait_send())
-        for h in range(PARTS):
-            loop(0, S, lambda e: t_copy(d, e, h).wait_send())
-            loop(1, S, lambda e: x_copy(d, e, h).wait_send())
-            if d > 0:
-                z_copy(d, h).wait_send()
-        for k in range(2):
-            v_copy(d, k).wait_send()
-            if d > 0:
-                h_copy(d, k).wait_send()
-            loop(1, S, lambda e: r_copy(d, e, k).wait_send())
+    sent(gate_send.at[pl.ds(1, Q - 1)], gate_ss.at[0])
+    sent(gate_send.at[0, pl.ds(1, S - 1)], gate_ss.at[1])
+    sent(sendz, z_ss)
+    sent(gathered.at[:, c, :, pl.ds(1, S - 1)], x_ss)
+    sent(gathered.at[:, c], t_ss)
+    sent(hidden.at[:, :, 0], v_ss)
+    sent(r_send, r_ss)
+    sent(home_send, h_ss)
     sq_copy.wait()
     norm = lax.rsqrt((squares + sq_recv[:, 0:1]) / width + EPS)
     out_ref[...] = (total * norm * out_gain_ref[...]).astype(BF16)
@@ -377,7 +368,7 @@
     dma = pltpu.SemaphoreType.DMA
     return pl.pallas_call(
         functools.partial(kernel, Q, S, R),
-        out_shape=jax.ShapeDtypeStruct((tok, H), BF16),
+        out_shape=pltpu.VMEM((tok, H), BF16),
         in_specs=[hbm] * 8,
         out_specs=vmem,
         scratch_shapes=[
@@ -386,28 +377,26 @@
             pltpu.VMEM((1, D), F32),
             pltpu.VMEM((1, H), F32),
             pltpu.VMEM((tok, D), BF16),
-            pltpu.VMEM((Q, PARTS, RC, D // PARTS), BF16),
+            pltpu.VMEM((Q - 1, PARTS, RC, D // PARTS), BF16),
             pltpu.VMEM((Q, K, PARTS, S, RC, D // PARTS), BF16),
             pltpu.VMEM((Q, K, tok, RC), BF16),
             pltpu.VMEM((Q, S, L, lanes), F32),
             pltpu.VMEM((Q, S, L, lanes), F32),
             pltpu.VMEM((L, D, F), BF16),
             pltpu.VMEM((L, D, F), BF16),
-            pltpu.VMEM((2, L * F, H), BF16),
-            pltpu.VMEM((L * F, H), BF16),
+            pltpu.VMEM((2, L, F, H), BF16),
+            pltpu.VMEM((L, F, H), BF16),
             pltpu.VMEM((Q, K, 2, S * RC, L * F), BF16),
-            pltpu.VMEM((Q, K, S, RC, H), BF16),
+            pltpu.VMEM((Q, K, S - 1, RC, H), BF16),
             pltpu.VMEM((Q, K, RC, H), F32),
-            pltpu.VMEM((Q, K, S, RC, H), BF16),
-            pltpu.VMEM((Q, K, RC, H), BF16),
+            pltpu.VMEM((Q, K, S - 1, RC, H), BF16),
+            pltpu.VMEM((Q - 1, K, RC, H), BF16),
             pltpu.VMEM((Q, K, RC, H), BF16),
             pltpu.VMEM((tok, H), F32),
             pltpu.VMEM((tok, 128), F32),
             pltpu.VMEM((tok, 128), F32),
-            dma((5,)), dma((4, L)), dma((Q, S)), dma((Q, S)), dma((Q, PARTS)), dma((Q, PARTS)),
-            dma((Q, S, PARTS)), dma((Q, S, PARTS)), dma((Q, S, PARTS)), dma((Q, S, PARTS)), dma, dma,
-            dma((Q, K)), dma((Q, K)), dma((Q, S, K)), dma((Q, S, K)), dma((Q, K)), dma((Q, K)),
-            dma, dma,
+            dma((5,)), dma((4,)), dma((2,)), dma((Q,)), dma, dma((Q - 1, PARTS)), dma, dma((Q, S - 1, PARTS)),
+            dma, dma((Q,)), dma, dma, dma, dma((Q, K)), dma, dma((Q, K)), dma, dma((Q - 1, K)), dma, dma,
         ],
         compiler_params=pltpu.CompilerParams(
             collective_id=0, has_side_effects=True, vmem_limit_bytes=64 * 1000 * 1000

time: 44.4 us -> 39.3 us (0.89)
  Pallas kernels: 42.5 us -> 38 us
  local copies, waits for them, and re-layouts: 1.67 us -> 0.71 us
    pallas_call x1, Pallas kernels: 42.5 us -> 38 us  [body(): pl.pallas_call(functools.partial(kernel, Q, S, R), out_shape=pltpu.VMEM((...]
    unnamed x1, local copies, waits for them, and re-layouts: 1.67 us -> 0.71 us
where the time goes in v3:
time: 39.3 us; the launch traced here: 38.8 us
  Pallas kernels  38 us (97%)
  local copies, waits for them, and re-layouts  0.71 us (2%)
    pallas_call x1, Pallas kernels, body(): pl.pallas_call(functools.partial(kernel, Q, S, R), out_shape=pltpu.VMEM((...  38 us

profile of v3, /device:TPU:0, one launch (start us, length us, event | category | flops | bytes accessed | tf_op | source)
XLA Modules:
  0.0 38.8 jit_solution(17689513691497871910)
XLA Ops:
  0.0 38.0 %shard_map.82 = bf16[128,1024]{1,0:T(8,128)(2,1)S(1)} custom-call(s32[4,128]{1,0:T(4,128)} %bitcast.6, f32[4,128]{1,0:T(4,128)} %bitcast.7, f32[1,2048]{1,0:T(1,128)} %bitcast.4, f32[1,1024]{1,0:T(1,128)} %bitcast.5, bf16[128,2048]{1,0:T(8,128)(2,1)} %tokens_hbm.1, bf16[2,2048,256]{2,1,0:T(8,128)(2,1)} %gate_hbm.1, bf16[2,2048,256]{2,1,0:T(8,128)(2,1)} %up_hbm.1, ...), custom_call_target="tpu_custom_call" | custom-call | tf_op jit(solution)/shard_map/pallas_call | solution.py:369
  38.0 0.7 %copy.10 = bf16[128,1024]{1,0:T(8,128)(2,1)} copy(bf16[128,1024]{1,0:T(8,128)(2,1)S(1)} %shard_map.82) | data formatting | bytes 524288

commit v4 on v3

--- a/solution.py
+++ b/solution.py
@@ -14,13 +14,13 @@
 BF16 = jnp.bfloat16
 
 STEPS = (
-    "B00", "A11", "A31", "B11", "G00", "B01", "A10", "A30", "G11", "A21", "B10", "D11",
-    "G10", "B30", "D10", "B31", "A20", "B21", "G30", "F11", "G21", "D30", "D21", "G31",
-    "B20", "F10", "D31", "G20", "F30", "D20", "F21", "G01", "F31", "D00", "D01", "F20",
-    "M10", "M30", "M21", "F00", "M00", "M11", "F01", "M01", "M20", "M31",
+    "A21", "B01", "A31", "B00", "A20", "B21", "G01", "A30", "G21", "G00", "A11", "B20",
+    "D21", "G20", "B31", "B30", "A10", "G30", "B11", "D20", "D30", "F21", "G11", "G31",
+    "B10", "D11", "F20", "D31", "G10", "F30", "D10", "F11", "F31", "D01", "D00", "F10",
+    "M30", "M21", "F00", "M00", "M20", "M11", "F01", "M01", "M10", "M31",
 )
-PLACES = ((3, 2, 1), (2, 3, 1), (2, 3, 1), (3, 2, 1))
-ORDERS = ((3, 2, 1), (2, 1, 3), (2, 3, 1), (3, 2, 1))
+PLACES = ((2, 3, 1), (3, 2, 1), (3, 2, 1), (2, 3, 1))
+ORDERS = ((3, 2, 1), (1, 2, 3), (2, 3, 1), (3, 2, 1))
 PARTS = 2
 
 
@@ -190,35 +190,41 @@
 
     for h in range(PARTS):
         forward(0, h)
-    for d in order:
+    def leave(d):
         for h in range(PARTS):
             z_copy(d, h).start()
+
+    for d in order[:-1]:
+        leave(d)
+
+    small[2].wait()
+    small[3].wait()
+    ids = lax.broadcasted_iota(jnp.int32, (-(-Q * group_width // 16) * 16, tok), 0)
+    dense = jnp.zeros(ids.shape, F32)
+    for k in range(top):
+        dense += jnp.where(routes_ref[k:k + 1, :] == ids, probs_ref[k:k + 1, :], 0.0)
+    coarse = dense.astype(BF16)
+    fine = (dense - coarse.astype(F32)).astype(BF16)
+    for d in range(Q):
+        pick = picks[d].astype(BF16)
+        lines = sum(
+            lax.dot_general(part, pick, (((1,), (1,)), ((), ())), preferred_element_type=F32) for part in (coarse, fine))
+        base = partner(q, d, Q)[0]
+        mine = jnp.zeros((group_width, lanes), F32)
+        for g in range(Q):
+            mine = jnp.where(base == g, lines[g * group_width:(g + 1) * group_width], mine)
+        for i in range(S):
+            gate_send[d, i] = mine[i * L:(i + 1) * L]
+    gate_recv[0, 0] = gate_send[0, s]
+    for d in range(Q):
+        loop(1 if d == 0 else 0, S, lambda e: gate_copy(d, e, int(d == 0)).start())
+    leave(order[-1])
     away.wait()
     u_copy().start()
 
-    small[2].wait()
-    small[3].wait()
-    for d in range(Q):
-        base = partner(q, d, Q)[0] * group_width
-        ids = base + lax.broadcasted_iota(jnp.int32, (-(-group_width // 8) * 8, tok), 0)
-        dense = jnp.zeros(ids.shape, F32)
-        for k in range(top):
-            dense += jnp.where(routes_ref[k:k + 1, :] == ids, probs_ref[k:k + 1, :], 0.0)
-        lines = lax.dot_general(
-            dense, picks[d], (((1,), (1,)), ((), ())),
-            precision=lax.Precision.HIGHEST, preferred_element_type=F32,
-        )
-        for i in range(S):
-            gate_send[d, i] = lines[i * L:(i + 1) * L]
-    gate_recv[0, 0] = gate_send[0, s]
-    for d in range(Q):
-        loop(1 if d == 0 else 0, S, lambda e: gate_copy(d, e, int(d == 0)).start())
-
     for d in range(Q):
         for k in range(2):
             unpack[d, k] = picks[d][k * RC:(k + 1) * RC].T.astype(BF16)
-    for copy in weights:
-        copy.wait()
 
     row, lane = (lax.broadcasted_iota(jnp.int32, (RC, lanes), i) for i in (0, 1))
 
@@ -271,6 +277,9 @@
 
     def step_g(p, k):
         d = place[p]
+        if not gates_ready:
+            for copy in weights:
+                copy.wait()
         if p not in gates_ready:
             arrived(gate_recv.at[d, pl.ds(1, S - 1)] if p == 0 else gate_recv.at[d], gate_rs.at[d])
             gates_ready.append(p)

time: 39.3 us -> 37.3 us (0.949)
  Pallas kernels: 38 us -> 36.2 us
    pallas_call x1, Pallas kernels: 38 us -> 36.2 us  [body(): pl.pallas_call(functools.partial(kernel, Q, S, R), out_shape=pltpu.VMEM((...]
where the time goes in v4:
time: 37.3 us; the launch traced here: 37 us
  Pallas kernels  36.2 us (97%)
  local copies, waits for them, and re-layouts  0.71 us (2%)
    pallas_call x1, Pallas kernels, body(): pl.pallas_call(functools.partial(kernel, Q, S, R), out_shape=pltpu.VMEM((...  36.2 us

profile of v4, /device:TPU:0, one launch (start us, length us, event | category | flops | bytes accessed | tf_op | source)
XLA Modules:
  0.0 37.0 jit_solution(16678312718414733213)
XLA Ops:
  0.0 36.2 %shard_map.82 = bf16[128,1024]{1,0:T(8,128)(2,1)S(1)} custom-call(s32[4,128]{1,0:T(4,128)} %bitcast.6, f32[4,128]{1,0:T(4,128)} %bitcast.7, f32[1,2048]{1,0:T(1,128)} %bitcast.4, f32[1,1024]{1,0:T(1,128)} %bitcast.5, bf16[128,2048]{1,0:T(8,128)(2,1)} %tokens_hbm.1, bf16[2,2048,256]{2,1,0:T(8,128)(2,1)} %gate_hbm.1, bf16[2,2048,256]{2,1,0:T(8,128)(2,1)} %up_hbm.1, ...), custom_call_target="tpu_custom_call" | custom-call | tf_op jit(solution)/shard_map/pallas_call | solution.py:378
  36.3 0.7 %copy.10 = bf16[128,1024]{1,0:T(8,128)(2,1)} copy(bf16[128,1024]{1,0:T(8,128)(2,1)S(1)} %shard_map.82) | data formatting | bytes 524288

commit v5 on v4

--- a/solution.py
+++ b/solution.py
@@ -14,14 +14,14 @@
 BF16 = jnp.bfloat16
 
 STEPS = (
-    "A21", "B01", "A31", "B00", "A20", "B21", "G01", "A30", "G21", "G00", "A11", "B20",
-    "D21", "G20", "B31", "B30", "A10", "G30", "B11", "D20", "D30", "F21", "G11", "G31",
-    "B10", "D11", "F20", "D31", "G10", "F30", "D10", "F11", "F31", "D01", "D00", "F10",
-    "M30", "M21", "F00", "M00", "M20", "M11", "F01", "M01", "M10", "M31",
+    "B01", "A20", "A21", "A30", "B00", "A31", "B21", "G21", "B20", "A11", "B31", "D21",
+    "G20", "A10", "B11", "G31", "B30", "D20", "F21", "G11", "D31", "B10", "G30", "D11",
+    "F20", "G10", "D30", "G00", "F31", "D10", "F11", "G01", "F30", "D00", "D01", "F10",
+    "F00", "M20", "M11", "M31", "M00", "M21", "F01", "M01", "M10", "M30",
 )
 PLACES = ((2, 3, 1), (3, 2, 1), (3, 2, 1), (2, 3, 1))
-ORDERS = ((3, 2, 1), (1, 2, 3), (2, 3, 1), (3, 2, 1))
-PARTS = 2
+ORDERS = ((3, 2, 1), (2, 1, 3), (2, 1, 3), (3, 2, 1))
+PARTS = 4
 
 
 def loop(low, high, step):

time: 37.3 us -> 36.9 us (0.989)
  Pallas kernels: 36.2 us -> 35.6 us
    pallas_call x1, Pallas kernels: 36.2 us -> 35.6 us  [body(): pl.pallas_call(functools.partial(kernel, Q, S, R), out_shape=pltpu.VMEM((...]
where the time goes in v5:
time: 36.9 us; the launch traced here: 36.3 us
  Pallas kernels  35.6 us (96%)
  local copies, waits for them, and re-layouts  0.71 us (2%)
    pallas_call x1, Pallas kernels, body(): pl.pallas_call(functools.partial(kernel, Q, S, R), out_shape=pltpu.VMEM((...  35.6 us

profile of v5, /device:TPU:0, one launch (start us, length us, event | category | flops | bytes accessed | tf_op | source)
XLA Modules:
  0.0 36.3 jit_solution(14578866012268791070)
XLA Ops:
  0.0 35.6 %shard_map.82 = bf16[128,1024]{1,0:T(8,128)(2,1)S(1)} custom-call(s32[4,128]{1,0:T(4,128)} %bitcast.6, f32[4,128]{1,0:T(4,128)} %bitcast.7, f32[1,2048]{1,0:T(1,128)} %bitcast.4, f32[1,1024]{1,0:T(1,128)} %bitcast.5, bf16[128,2048]{1,0:T(8,128)(2,1)} %tokens_hbm.1, bf16[2,2048,256]{2,1,0:T(8,128)(2,1)} %gate_hbm.1, bf16[2,2048,256]{2,1,0:T(8,128)(2,1)} %up_hbm.1, ...), custom_call_target="tpu_custom_call" | custom-call | tf_op jit(solution)/shard_map/pallas_call | solution.py:378
  35.6 0.7 %copy.10 = bf16[128,1024]{1,0:T(8,128)(2,1)} copy(bf16[128,1024]{1,0:T(8,128)(2,1)S(1)} %shard_map.82) | data formatting | bytes 524288

commit v6 on v5

--- a/solution.py
+++ b/solution.py
@@ -17,7 +17,7 @@
     "B01", "A20", "A21", "A30", "B00", "A31", "B21", "G21", "B20", "A11", "B31", "D21",
     "G20", "A10", "B11", "G31", "B30", "D20", "F21", "G11", "D31", "B10", "G30", "D11",
     "F20", "G10", "D30", "G00", "F31", "D10", "F11", "G01", "F30", "D00", "D01", "F10",
-    "F00", "M20", "M11", "M31", "M00", "M21", "F01", "M01", "M10", "M30",
+    "F00", "F01", "M20", "M11", "M31", "M00", "M21", "M01", "M10", "M30",
 )
 PLACES = ((2, 3, 1), (3, 2, 1), (3, 2, 1), (2, 3, 1))
 ORDERS = ((3, 2, 1), (2, 1, 3), (2, 1, 3), (3, 2, 1))
@@ -92,15 +92,16 @@
             (routes_hbm, routes_ref), (in_gain_hbm, in_gain_ref), (probs_hbm, probs_ref), (out_gain_hbm, out_gain_ref)))
     ]
     tok_copy = pltpu.make_async_copy(tokens_hbm, tokens_ref, tok_sem.at[4])
+    tok_copy.start()
     small[0].start()
-    tok_copy.start()
+
+    barrier = pltpu.get_barrier_semaphore()
+    for d in reversed(range(Q)):
+        loop(1 if d == 0 else 0, S, lambda e: pl.semaphore_signal(
+            barrier, inc=1, device_id=at(partner(q, d, Q)[0] * S + lax.rem(s + e, S)), device_id_type=MESH))
+    pl.semaphore_signal(barrier, inc=1, device_id=at(me, 1 - c), device_id_type=MESH)
     for copy in small[1:]:
         copy.start()
-
-    barrier = pltpu.get_barrier_semaphore()
-    loop(1, N, lambda p: pl.semaphore_signal(
-        barrier, inc=1, device_id=at(lax.rem(me + p, N)), device_id_type=MESH))
-    pl.semaphore_signal(barrier, inc=1, device_id=at(me, 1 - c), device_id_type=MESH)
 
     own_cols = pl.ds(pl.multiple_of(c * H, H), H)
     other_cols = pl.ds(pl.multiple_of((1 - c) * H, H), H)
@@ -190,6 +191,10 @@
 
     for h in range(PARTS):
         forward(0, h)
+    def q_copy(d, k, p):
+        home = at(me, 1 - c) if p == 0 else at(partner(q, d, Q)[1] * S + s, 1 - c)
+        return remote(sq_send.at[d, k], sq_recv.at[d, k], q_ss, q_rs.at[d, k], home)
+
     def leave(d):
         for h in range(PARTS):
             z_copy(d, h).start()
@@ -255,7 +260,23 @@
     def sent(block, sem):
         remote(block, block, sem, sem, at(me, 1 - c)).wait_send()
 
-    down_ready, gates_ready, mixed_ready = [], [], []
+    ups_left = [(p, k) for p in range(Q) for k in range(2)]
+    down_ready, gates_ready, mixed_ready, unsent = [], [], [], []
+
+    def send_squares():
+        units = list(unsent)
+        unsent.clear()
+        for p, k in units:
+            d = place[p]
+            rows = (home_recv[0, k] if p == 0 else home_send[d - 1, k]).astype(F32)
+            squares = rows * rows
+            squares = sum(squares[:, i:i + 128] for i in range(128, H, 128)) + squares[:, :128]
+            line = lax.dot_general(
+                jnp.ones((8, 128), F32), squares, (((1,), (1,)), ((), ())),
+                precision=lax.Precision.HIGHEST, preferred_element_type=F32)
+            sq_send[d, k, :, :RC] = line[:1]
+        for p, k in units:
+            q_copy(place[p], k, p).start()
 
     def step_a(p, k):
         d = place[p]
@@ -277,6 +298,7 @@
 
     def step_g(p, k):
         d = place[p]
+        ups_left.remove((p, k))
         if not gates_ready:
             for copy in weights:
                 copy.wait()
@@ -290,6 +312,7 @@
         else:
             lax.fori_loop(0, S // pair, lambda n, carry: (up_projection(d, k, n), carry)[1], 0)
         v_copy(d, k).start()
+        send_squares()
 
     def step_d(p, k):
         d = place[p]
@@ -323,6 +346,9 @@
         else:
             home_send[d - 1, k] = total.astype(BF16)
             h_copy(d, k).start()
+        unsent.append((p, k))
+        if not ups_left:
+            send_squares()
 
     def step_m(p, k):
         d = place[p]
@@ -343,9 +369,6 @@
 
     total = mixed[...]
     squares = jnp.sum(total * total, axis=1, keepdims=True)
-    sq_send[...] = jnp.broadcast_to(squares, sq_send.shape)
-    sq_copy = remote(sq_send, sq_recv, q_ss, q_rs, at(me, 1 - c))
-    sq_copy.start()
     u_copy().wait_send()
     sent(gate_send.at[pl.ds(1, Q - 1)], gate_ss.at[0])
     sent(gate_send.at[0, pl.ds(1, S - 1)], gate_ss.at[1])
@@ -355,9 +378,14 @@
     sent(hidden.at[:, :, 0], v_ss)
     sent(r_send, r_ss)
     sent(home_send, h_ss)
-    sq_copy.wait()
-    norm = lax.rsqrt((squares + sq_recv[:, 0:1]) / width + EPS)
-    out_ref[...] = (total * norm * out_gain_ref[...]).astype(BF16)
+    sent(sq_send, q_ss)
+    theirs = jnp.zeros((tok, RC), F32)
+    for p in range(Q):
+        for k in range(2):
+            q_copy(place[p], k, p).wait_recv()
+            theirs += unpack[place[p], k].astype(F32) * sq_recv[place[p], k, :, :RC]
+    squares = squares + jnp.sum(theirs, axis=1, keepdims=True)
+    out_ref[...] = (total * lax.rsqrt(squares / width + EPS) * out_gain_ref[...]).astype(BF16)
 
 
 def body(tokens, in_gain, routing, gate_prob, w_gate, w_up, w_down, out_gain):
@@ -402,10 +430,10 @@
             pltpu.VMEM((Q - 1, K, RC, H), BF16),
             pltpu.VMEM((Q, K, RC, H), BF16),
             pltpu.VMEM((tok, H), F32),
-            pltpu.VMEM((tok, 128), F32),
-            pltpu.VMEM((tok, 128), F32),
+            pltpu.VMEM((Q, K, 1, lanes), F32),
+            pltpu.VMEM((Q, K, 1, lanes), F32),
             dma((5,)), dma((4,)), dma((2,)), dma((Q,)), dma, dma((Q - 1, PARTS)), dma, dma((Q, S - 1, PARTS)),
-            dma, dma((Q,)), dma, dma, dma, dma((Q, K)), dma, dma((Q, K)), dma, dma((Q - 1, K)), dma, dma,
+            dma, dma((Q,)), dma, dma, dma, dma((Q, K)), dma, dma((Q, K)), dma, dma((Q - 1, K)), dma, dma((Q, K)),
         ],
         compiler_params=pltpu.CompilerParams(
             collective_id=0, has_side_effects=True, vmem_limit_bytes=64 * 1000 * 1000

time: 36.9 us -> 36.7 us (level); the launches traced: 36.3 us -> 36.6 us
  no operation moved by 1% of the time
where the time goes in v6:
time: 36.7 us; the launch traced here: 36.6 us
  Pallas kernels  35.9 us (98%)
  local copies, waits for them, and re-layouts  0.71 us (2%)
    pallas_call x1, Pallas kernels, body(): pl.pallas_call(functools.partial(kernel, Q, S, R), out_shape=pltpu.VMEM((...  35.9 us

profile of v6, /device:TPU:0, one launch (start us, length us, event | category | flops | bytes accessed | tf_op | source)
XLA Modules:
  0.0 36.6 jit_solution(16146822838303250250)
XLA Ops:
  0.0 35.9 %shard_map.82 = bf16[128,1024]{1,0:T(8,128)(2,1)S(1)} custom-call(s32[4,128]{1,0:T(4,128)} %bitcast.6, f32[4,128]{1,0:T(4,128)} %bitcast.7, f32[1,2048]{1,0:T(1,128)} %bitcast.4, f32[1,1024]{1,0:T(1,128)} %bitcast.5, bf16[128,2048]{1,0:T(8,128)(2,1)} %tokens_hbm.1, bf16[2,2048,256]{2,1,0:T(8,128)(2,1)} %gate_hbm.1, bf16[2,2048,256]{2,1,0:T(8,128)(2,1)} %up_hbm.1, ...), custom_call_target="tpu_custom_call" | custom-call | tf_op jit(solution)/shard_map/pallas_call | solution.py:406
  35.9 0.7 %copy.10 = bf16[128,1024]{1,0:T(8,128)(2,1)} copy(bf16[128,1024]{1,0:T(8,128)(2,1)S(1)} %shard_map.82) | data formatting | bytes 524288

commit v7 on v6

--- a/solution.py
+++ b/solution.py
@@ -14,13 +14,13 @@
 BF16 = jnp.bfloat16
 
 STEPS = (
-    "B01", "A20", "A21", "A30", "B00", "A31", "B21", "G21", "B20", "A11", "B31", "D21",
-    "G20", "A10", "B11", "G31", "B30", "D20", "F21", "G11", "D31", "B10", "G30", "D11",
-    "F20", "G10", "D30", "G00", "F31", "D10", "F11", "G01", "F30", "D00", "D01", "F10",
-    "F00", "F01", "M20", "M11", "M31", "M00", "M21", "M01", "M10", "M30",
+    "A20", "B00", "A21", "A30", "A31", "B21", "G21", "B20", "A11", "B31", "D21", "G20",
+    "A10", "B11", "G31", "B30", "D20", "G11", "F21", "D31", "G30", "B10", "B01", "D11",
+    "D30", "F20", "G10", "F31", "G00", "D10", "F11", "G01", "F30", "D00", "D01", "F10",
+    "M31", "M20", "F00", "F01", "M11", "M00", "M21", "M01", "M30", "M10",
 )
 PLACES = ((2, 3, 1), (3, 2, 1), (3, 2, 1), (2, 3, 1))
-ORDERS = ((3, 2, 1), (2, 1, 3), (2, 1, 3), (3, 2, 1))
+ORDERS = ((3, 2, 1), (1, 2, 3), (1, 2, 3), (3, 2, 1))
 PARTS = 4
 
 

time: 36.7 us -> 36.4 us (level); the launches traced: 36.6 us -> 35.9 us
  Pallas kernels: 35.9 us -> 35.2 us
    pallas_call x1, Pallas kernels: 35.9 us -> 35.2 us  [body(): pl.pallas_call(functools.partial(kernel, Q, S, R), out_shape=pltpu.VMEM((...]
where the time goes in v7:
time: 36.4 us; the launch traced here: 35.9 us
  Pallas kernels  35.2 us (97%)
  local copies, waits for them, and re-layouts  0.71 us (2%)
    pallas_call x1, Pallas kernels, body(): pl.pallas_call(functools.partial(kernel, Q, S, R), out_shape=pltpu.VMEM((...  35.2 us

profile of v7, /device:TPU:0, one launch (start us, length us, event | category | flops | bytes accessed | tf_op | source)
XLA Modules:
  0.0 35.9 jit_solution(10000252530897908231)
XLA Ops:
  0.0 35.2 %shard_map.82 = bf16[128,1024]{1,0:T(8,128)(2,1)S(1)} custom-call(s32[4,128]{1,0:T(4,128)} %bitcast.6, f32[4,128]{1,0:T(4,128)} %bitcast.7, f32[1,2048]{1,0:T(1,128)} %bitcast.4, f32[1,1024]{1,0:T(1,128)} %bitcast.5, bf16[128,2048]{1,0:T(8,128)(2,1)} %tokens_hbm.1, bf16[2,2048,256]{2,1,0:T(8,128)(2,1)} %gate_hbm.1, bf16[2,2048,256]{2,1,0:T(8,128)(2,1)} %up_hbm.1, ...), custom_call_target="tpu_custom_call" | custom-call | tf_op jit(solution)/shard_map/pallas_call | solution.py:406
  35.2 0.7 %copy.10 = bf16[128,1024]{1,0:T(8,128)(2,1)} copy(bf16[128,1024]{1,0:T(8,128)(2,1)S(1)} %shard_map.82) | data formatting | bytes 524288
